TPU v7x, 32 devices: a whole 2x2x4 slice. The times are simulated.
32 devices in a mesh: ep: 8 (over z, x), tp: 4 (over y, core).
Axes of the slice: x: 2, y: 2, z: 4, core: 2. Of those that a mesh axis runs over, the one named last changes fastest.
Arguments:
- queries: bfloat16 [2048, 2, 1024], P('ep', None, 'tp')
- keys: bfloat16 [2048, 2, 256], P('ep', None, 'tp')
- values: bfloat16 [2048, 2, 256], P('ep', None, 'tp'), may hold values from -6 to 6
- query_gain: float32 [64], replicated, may hold values from 1.2 to 6
- key_gain: float32 [64], replicated, may hold values from 1.2 to 6
- out_weight: bfloat16 [1024, 2048], P('tp'), may hold values from -0.75 to 0.75
- moe_tokens: bfloat16 [4096, 2048], P(('ep', 'tp')), may hold values from -6 to 6
- moe_gain: float32 [2048], replicated, may hold values from 0.1 to 1.9
- routes: int32 [4096, 2], P(('ep', 'tp')), may hold values from 0 to 7, all different within a row; in each aligned block of 128 rows (0 to 127, 128 to 255, ...) at most 48 rows name the same one
- route_weight: float32 [4096, 2], P(('ep', 'tp')), may hold values from 0.1 to 1
- w_gate: bfloat16 [8, 2048, 1024], P('ep', None, 'tp'), may hold values from -0.125 to 0.125
- w_up: bfloat16 [8, 2048, 1024], P('ep', None, 'tp'), may hold values from -0.125 to 0.125
- w_down: bfloat16 [8, 1024, 2048], P('ep', 'tp'), may hold values from -0.1875 to 0.1875
Outputs:
- attended: bfloat16 [2048, 2, 2048], P(('ep', 'tp'))
- routed: bfloat16 [4096, 2048], P(('ep', 'tp'))
Inputs may be any that keep to these rules, and one draw needn't show every extreme that they name: `routes`: each row names 2 different experts. The rows of one device name no expert more than 48 times, and in every draw some device's rows name one expert exactly 48 times.
All inputs are finite; a program needn't handle non-finite values.
Results may differ from a plain program's by a relative error of at most 0.013.
The roundings to bfloat16 on the way count: a program that leaves them out, or rounds other values in their place, can miss the bound.
Values may be sent and summed in bfloat16 or wider, within the bound.
A program may use at most 128 MiB of HBM per device.

v0:
```python
import math

import jax
import jax.numpy as jnp
from jax import lax
from jax.sharding import PartitionSpec as P

HEAD_DIM = 64
GRID_W = 64


EPS = 1e-06
THETA = 10000.0


def turn(normed, positions):
    quarter = normed.shape[-1] // 4
    inverse = THETA ** (-jnp.arange(quarter, dtype=jnp.float32) / quarter)
    grid_row = (positions // GRID_W).astype(jnp.float32)
    grid_col = (positions % GRID_W).astype(jnp.float32)
    angles = jnp.stack([grid_row[:, None] * inverse, grid_col[:, None] * inverse], axis=1)
    cosine = jnp.cos(angles)[:, None, None]
    sine = jnp.sin(angles)[:, None, None]
    parts = normed.reshape(normed.shape[:-1] + (2, 2, quarter))
    first = parts[..., 0, :]
    second = parts[..., 1, :]
    turned = jnp.stack([first * cosine - second * sine, second * cosine + first * sine], axis=-2)
    return turned.reshape(normed.shape)


def prepare(data, positions, gain):
    heads = data.astype(jnp.float32).reshape(data.shape[0], data.shape[1], -1, HEAD_DIM)
    normed = heads * lax.rsqrt(jnp.mean(heads * heads, axis=-1, keepdims=True) + EPS) * gain
    return turn(normed, positions).astype(jnp.bfloat16)


def per_device(
    queries,
    keys,
    values,
    query_gain,
    key_gain,
    out_weight,
    moe_tokens,
    moe_gain,
    routes,
    route_weight,
    w_gate,
    w_up,
    w_down,
):
    pos_count = queries.shape[0]
    seq_count = queries.shape[1]
    positions = lax.axis_index("ep") * pos_count + jnp.arange(pos_count, dtype=jnp.int32)
    q_rot = prepare(queries, positions, query_gain)
    k_rot = prepare(keys, positions, key_gain)
    kv_local = k_rot.shape[2]
    groups = q_rot.shape[2] // kv_local
    value_heads = values.reshape(pos_count, seq_count, kv_local, HEAD_DIM)
    q_group = q_rot.reshape(pos_count, seq_count, kv_local, groups, HEAD_DIM)
    scale = HEAD_DIM ** (-0.5)
    start_state = (
        jnp.full((seq_count, kv_local, groups, pos_count), -1e30, jnp.float32),
        jnp.zeros((seq_count, kv_local, groups, pos_count), jnp.float32),
        jnp.zeros((pos_count, seq_count, kv_local, groups, HEAD_DIM), jnp.float32),
    )
    carry = start_state
    key_piece = lax.all_gather(k_rot, "ep", axis=0, tiled=True)
    value_piece = lax.all_gather(value_heads, "ep", axis=0, tiled=True)
    count = key_piece.shape[0]
    width = math.gcd(count, 512)
    key_split = key_piece.reshape(count // width, width, seq_count, kv_local, HEAD_DIM)
    value_split = value_piece.reshape(count // width, width, seq_count, kv_local, HEAD_DIM)

    def step(state, block):
        best, total, accum = state
        key_block, value_block = block
        scores = (
            jnp.einsum("pskgd,lskd->skgpl", q_group, key_block, preferred_element_type=jnp.float32)
            * scale
        )
        new_best = jnp.maximum(best, jnp.max(scores, axis=-1))
        factor = jnp.exp(best - new_best)
        expo = jnp.exp(scores - new_best[..., None])
        total = total * factor + jnp.sum(expo, axis=-1)
        added = jnp.einsum(
            "skgpl,lskd->pskgd",
            expo.astype(jnp.bfloat16),
            value_block,
            preferred_element_type=jnp.float32,
        )
        accum = accum * jnp.transpose(factor, (3, 0, 1, 2))[..., None] + added
        return ((new_best, total, accum), None)

    carry, _ = lax.scan(step, carry, (key_split, value_split))
    best, total, accum = carry
    mixed = (accum / jnp.transpose(total, (3, 0, 1, 2))[..., None]).astype(jnp.bfloat16)
    mixed = mixed.reshape(pos_count, seq_count, -1)
    rows = mixed
    product = jnp.dot(
        rows.reshape(pos_count // lax.axis_size("tp") * lax.axis_size("tp") * seq_count, -1),
        out_weight,
        preferred_element_type=jnp.float32,
    )
    attended = lax.psum_scatter(
        product.reshape(
            pos_count // lax.axis_size("tp") * lax.axis_size("tp"), seq_count, -1
        ).astype(jnp.bfloat16),
        "tp",
        scatter_dimension=0,
        tiled=True,
    )
    tok_count = moe_tokens.shape[0]
    top_count = routes.shape[1]
    experts = lax.axis_size("ep")
    capacity = max(2, (3 * tok_count * top_count + 2 * experts - 1) // (2 * experts))
    token_float = moe_tokens.astype(jnp.float32)
    normed = (
        token_float
        * lax.rsqrt(jnp.mean(token_float * token_float, axis=-1, keepdims=True) + EPS)
        * moe_gain
    ).astype(jnp.bfloat16)
    hits = (routes[:, :, None] == jnp.arange(experts, dtype=jnp.int32)[None, None, :]).astype(
        jnp.float32
    )
    pair_count = tok_count * top_count
    flat_hits = hits.reshape(pair_count, experts)
    pair_index = jnp.arange(pair_count, dtype=jnp.int32)
    earlier = (pair_index[:, None] > pair_index[None, :]).astype(jnp.float32)
    before = jnp.dot(earlier, flat_hits, precision=lax.Precision.HIGHEST)
    rank = jnp.sum(before * flat_hits, axis=-1).astype(jnp.int32).reshape(tok_count, top_count)
    slot = routes * capacity + rank
    table = jnp.arange(experts * capacity, dtype=jnp.int32)
    dispatch = jnp.sum(
        (slot[None, :, :] == table[:, None, None]).astype(jnp.float32), axis=2
    ).astype(jnp.bfloat16)
    send = jnp.dot(dispatch, normed, preferred_element_type=jnp.float32).astype(jnp.bfloat16)
    received = lax.all_to_all(send, "ep", split_axis=0, concat_axis=0, tiled=True)
    rows = lax.all_gather(received, "tp", axis=0, tiled=True)
    gate = jnp.dot(rows, w_gate[0], preferred_element_type=jnp.float32)
    up = jnp.dot(rows, w_up[0], preferred_element_type=jnp.float32)
    hidden = (jax.nn.silu(gate) * up).astype(jnp.bfloat16)
    rows = hidden
    result = lax.psum_scatter(
        jnp.dot(rows, w_down[0], preferred_element_type=jnp.float32).astype(jnp.bfloat16),
        "tp",
        scatter_dimension=0,
        tiled=True,
    )
    returned_rows = lax.all_to_all(result, "ep", split_axis=0, concat_axis=0, tiled=True)
    combined = jnp.zeros((tok_count, returned_rows.shape[-1]), jnp.float32)
    for choice_index in range(top_count):
        picker = (slot[:, choice_index : choice_index + 1] == table[None, :]).astype(jnp.bfloat16)
        picked = jnp.dot(picker, returned_rows, preferred_element_type=jnp.float32)
        combined = combined + picked * route_weight[:, choice_index : choice_index + 1]
    return (attended, combined.astype(jnp.bfloat16))


def solution(mesh):
    in_specs = (
        P("ep", None, "tp"),
        P("ep", None, "tp"),
        P("ep", None, "tp"),
        P(),
        P(),
        P("tp", None),
        P(("ep", "tp"), None),
        P(),
        P(("ep", "tp"), None),
        P(("ep", "tp"), None),
        P("ep", None, "tp"),
        P("ep", None, "tp"),
        P("ep", "tp", None),
    )
    out_specs = (P(("ep", "tp"), None, None), P(("ep", "tp"), None))
    return jax.shard_map(
        per_device, mesh=mesh, in_specs=in_specs, out_specs=out_specs, check_vma=False
    )
```

profile of v0, /device:TPU:0, one launch (start us, length us, event | category | flops | bytes accessed | tf_op | source)
XLA Modules:
  0.0 241.3 jit_solution(14699746552922616163)
XLA Ops:
  7.2 1.4 fusion.28
  8.6 0.8 copy.53
  10.0 0.7 multiply_add_fusion
  10.7 1.7 convolution_convert_fusion.2
  12.4 44.2 %all_to_all.24 = bf16[8,48,2048]{2,1,0:T(8,128)(2,1)} all-to-all(bf16[8,48,2048]{2,1,0:T(8,128)(2,1)S(1)} %bitcast.136), channel_id=1, replica_groups=mesh['ep'=8,'tp'=4] {'ep'}, dimensions={0} | all-to-all | bytes 3145728 | tf_op jit(solution)/shard_map/all_to_all | solution.py:138
  56.7 45.5 %all-gather.3.cloned.1.call-done = bf16[1536,2048]{1,0:T(8,128)(2,1)} async-done(((bf16[384,2048]{1,0:T(8,128)(2,1)}), bf16[1536,2048]{1,0:T(8,128)(2,1)}) %all-gather.3.cloned.1.call-update) | async-done | bytes 6291472 | tf_op jit(solution)/shard_map/all_gather | solution.py:139
  102.2 5.8 %fusion.34 = f32[1536,256]{1,0:T(8,128)} fusion(bf16[1536,2048]{1,0:T(8,128)(2,1)} %all-gather.3.cloned.1.call-done, bf16[1,2048,256]{2,1,0:T(8,128)(2,1)S(1)} %copy-done.7), kind=kOutput, calls=%fused_computation.44 | convolution fusion | flops 1610612736 | bytes 8912896 | tf_op jit(solution)/shard_map/dot_general | solution.py:140
  108.0 12.3 %convolution_convert_fusion = bf16[1536,2048]{1,0:T(8,128)(2,1)} fusion(bf16[1536,2048]{1,0:T(8,128)(2,1)} %all-gather.3.cloned.1.call-done, f32[1536,256]{1,0:T(8,128)} %fusion.34, bf16[1,256,2048]{2,1,0:T(8,128)(2,1)S(1)} %copy-done, bf16[1,2048,256]{2,1,0:T(8,128)(2,1)S(1)} %copy-done.8), kind=kOutput, calls=%fused_computation.26 | convolution fusion | flops 3226730496 | bytes 16252928 | tf_op jit(solution)/shard_map/dot_general | solution.py:145
  120.4 0.5 copy-done.6
  121.0 0.2 copy-done.2
  121.9 31.5 %all_gather.9 = bf16[2048,2,1,64]{0,3,1,2:T(8,128)(2,1)S(1)} all-gather(bf16[256,2,1,64]{0,3,1,2:T(8,128)(2,1)S(1)} %bitcast.146), channel_id=1, replica_groups=mesh['ep'=8,'tp'=4] {'ep'}, dimensions={0}, use_global_device_ids=true | all-gather | bytes 589824 | tf_op jit(solution)/shard_map/all_gather | solution.py:68
  153.4 31.5 %all-gather = bf16[2048,2,64]{0,2,1:T(8,128)(2,1)S(1)} all-gather(bf16[256,2,64]{0,2,1:T(8,128)(2,1)S(1)} %copy-done.3), channel_id=2, replica_groups=mesh['ep'=8,'tp'=4] {'ep'}, dimensions={0}, use_global_device_ids=true | all-gather | bytes 589824 | tf_op jit(solution)/shard_map/all_gather | solution.py:69
  184.9 0.4 reshape.289
  185.7 10.0 %while.15 = (s32[]{:T(128)}, f32[2,1,4,256]{3,2,0,1:T(4,128)S(1)}, f32[2,1,4,256]{3,2,0,1:T(4,128)S(1)}, f32[256,2,1,4,64]{0,4,3,1,2:T(8,128)S(1)}, bf16[4,512,2...) while((s32[]{:T(128)}, f32[2,1,4,256]{3,2,0,1:T(4,128)S(1)}, ...), condition=%wide.region_5.6_spmd.clone, body=%wide.region_2.5_spmd.clone.sunk | while | flops 277229568 | bytes 14286969 | solution.py:95
  185.7 0.8 bitcast_reduce_fusion.3
  186.5 0.7 fusion.67
  187.2 0.9 fusion.68
  188.2 0.8 bitcast_reduce_fusion.3
  189.0 0.7 fusion.67
  189.7 0.9 fusion.68
  190.7 0.8 bitcast_reduce_fusion.3
  191.5 0.7 fusion.67
  192.2 0.9 fusion.68
  193.2 0.8 bitcast_reduce_fusion.3
  194.0 0.7 fusion.67
  194.7 0.9 fusion.68
  195.8 3.3 %convolution_convert_fusion.1 = bf16[256,2,2048]{2,0,1:T(8,128)(2,1)} fusion(bf16[256,2,256]{0,2,1:T(8,128)(2,1)S(1)} %bitcast.143, bf16[256,2048]{1,0:T(8,128)(2,1)} %param.20), kind=kOutput, calls=%fused_computation.27 | convolution fusion | flops 537919488 | bytes 3407872 | tf_op jit(solution)/shard_map/dot_general | solution.py:100
  199.1 5.7 %all-to-all-start.1 = ((bf16[8,48,2048]{2,1,0:T(8,128)(2,1)}), bf16[8,48,2048]{2,1,0:T(8,128)(2,1)S(1)}, u32[]{:S(2)}, u32[]{:S(2)}) async-start(bf16[8,48,2048]{2,1,0:T(8,128)(2,1)} %bitcast.142), calls=%async_computation.3 | async-start | bytes 3145728 | tf_op jit(solution)/shard_map/all_to_all | solution.py:150
  204.8 25.8 %reduce-scatter.3.cloned.1.call-done = bf16[64,2,2048]{2,0,1:T(8,128)(2,1)} async-done(((bf16[256,2,2048]{2,0,1:T(8,128)(2,1)}), bf16[64,2,2048]{2,0,1:T(8,128)(2,1)}) %reduce-scatter.3.cloned.1.call-update) | async-done | bytes 524304 | tf_op jit(solution)/shard_map/reduce_scatter | solution.py:105
  230.6 2.4 copy.55
  232.9 0.5 convolution_multiply_fusion.2
  233.4 1.3 fusion.26
  (67 shorter events, 2.1 us)
Async XLA Ops:
  7.2 100.8 %copy-start = (bf16[1,256,2048]{2,1,0:T(8,128)(2,1)S(1)}, bf16[1,256,2048]{2,1,0:T(8,128)(2,1)}, u32[]{:S(2)}) copy-start(bf16[1,256,2048]{2,1,0:T(8,128)(2,1)} %param.27) | copy-start | bytes 3145732
  7.2 95.0 %copy-start.7 = (bf16[1,2048,256]{2,1,0:T(8,128)(2,1)S(1)}, bf16[1,2048,256]{2,1,0:T(8,128)(2,1)}, u32[]{:S(2)}) copy-start(bf16[1,2048,256]{2,1,0:T(8,128)(2,1)} %param.25) | copy-start | bytes 3145732
  7.2 95.0 %all-gather.3.cloned.1.call-start = ((), (), s32[]{:S(2)}) async-start(), calls=%async_computation.5 | async-start | bytes 7864320 | tf_op jit(solution)/shard_map/all_gather | solution.py:139
  56.6 51.4 %copy-start.8 = (bf16[1,2048,256]{2,1,0:T(8,128)(2,1)S(1)}, bf16[1,2048,256]{2,1,0:T(8,128)(2,1)}, u32[]{:S(2)}) copy-start(bf16[1,2048,256]{2,1,0:T(8,128)(2,1)} %param.26) | copy-start | bytes 3145732
  56.7 142.5 %reduce-scatter.5.cloned.1.call-start = ((), (), s32[]{:S(2)}) async-start(), calls=%async_computation.6 | async-start | bytes 7864320 | tf_op jit(solution)/shard_map/reduce_scatter | solution.py:144
  120.3 0.7 copy-start.6
  120.3 1.0 copy-start.2
  120.3 1.4 copy-start.1
  120.3 1.4 copy-start.5
  120.3 33.1 %copy-start.3 = (bf16[256,2,64]{0,2,1:T(8,128)(2,1)S(1)}, bf16[256,2,64]{0,2,1:T(8,128)(2,1)}, u32[]{:S(2)}) copy-start(bf16[256,2,64]{0,2,1:T(8,128)(2,1)} %param.17) | copy-start | bytes 196612
  120.3 110.2 %reduce-scatter.3.cloned.1.call-start = ((), (), s32[]{:S(2)}) async-start(), calls=%async_computation.4 | async-start | bytes 2621440 | tf_op jit(solution)/shard_map/reduce_scatter | solution.py:105
  195.7 9.0 %copy-start.4 = (f32[128,2]{0,1:T(2,128)S(1)}, f32[128,2]{0,1:T(2,128)}, u32[]{:S(2)}) copy-start(f32[128,2]{0,1:T(2,128)} %param.24) | copy-start | bytes 3076
  199.1 33.8 %all-to-all-start.1 = ((bf16[8,48,2048]{2,1,0:T(8,128)(2,1)}), bf16[8,48,2048]{2,1,0:T(8,128)(2,1)S(1)}, u32[]{:S(2)}, u32[]{:S(2)}) async-start(bf16[8,48,2048]{2,1,0:T(8,128)(2,1)} %bitcast.142), calls=%async_computation.3 | async-start | bytes 3145728 | tf_op jit(solution)/shard_map/all_to_all | solution.py:150
Sparse Core Ops, SparseCore 0:
  56.8 45.3 all-gather.2
  120.5 58.8 reduce-scatter.4
  199.2 31.3 reduce-scatter.2
where the time goes:
time: 242 us; the launch traced here: 241 us
  blocking collectives  107 us (44%)
  waiting for transfers between devices  71.3 us (29%)
  matrix products  31.9 us (13%)
  between operations  14 us (6%)
  other arithmetic  5.82 us (2%)
  starting transfers between devices  5.78 us (2%)
  local copies, waits for them, and re-layouts  5.07 us (2%)
    all_gather x1, waiting for transfers between devices, per_device(): rows = lax.all_gather(received, 'tp', axis=0, tiled=True)  45.5 us
    all_to_all x1, blocking collectives, per_device(): lax.all_to_all(send, 'ep', split_axis=0, concat_axis=0, tiled=True)  44.2 us
    all_gather x1, blocking collectives, per_device(): value_piece = lax.all_gather(value_heads, 'ep', axis=0, tiled=True)  31.5 us
    all_gather x1, blocking collectives, per_device(): key_piece = lax.all_gather(k_rot, 'ep', axis=0, tiled=True)  31.5 us
    reduce_scatter x1, waiting for transfers between devices, per_device(): lax.psum_scatter(product.reshape(pos_count // lax.axis_size('tp') * lax.a...  25.8 us
    dot_general x1, matrix products, per_device(): jnp.dot(rows, w_down[0], preferred_element_type=jnp.float32)  12.3 us
    dot_general x1, matrix products, per_device(): gate = jnp.dot(rows, w_gate[0], preferred_element_type=jnp.float32)  5.8 us
    all_to_all x1, starting transfers between devices, per_device(): lax.all_to_all(result, 'ep', split_axis=0, concat_axis=0, tiled=True)  5.66 us
  transfers between devices with their start and end apart: 4, of which 2 were waited for; matrix products, arithmetic and copies ran while one was open for 7% of the time, Pallas kernels for 0%

commit v1 on v0

--- a/solution.py
+++ b/solution.py
@@ -1,8 +1,11 @@
+import functools
 import math
 
 import jax
 import jax.numpy as jnp
 from jax import lax
+from jax.experimental import pallas as pl
+from jax.experimental.pallas import tpu as pltpu
 from jax.sharding import PartitionSpec as P
 
 HEAD_DIM = 64
@@ -32,6 +35,272 @@
     heads = data.astype(jnp.float32).reshape(data.shape[0], data.shape[1], -1, HEAD_DIM)
     normed = heads * lax.rsqrt(jnp.mean(heads * heads, axis=-1, keepdims=True) + EPS) * gain
     return turn(normed, positions).astype(jnp.bfloat16)
+
+
+MESH = pl.DeviceIdType.MESH
+
+
+def greet(partners):
+    barrier = pltpu.get_barrier_semaphore()
+    for device in partners:
+        pl.semaphore_signal(barrier, inc=1, device_id=device, device_id_type=MESH)
+    pl.semaphore_wait(barrier, len(partners))
+
+
+def all_partners(e, t, experts):
+    low, high = t + 1 - 2 * (t % 2), (t + 2) % 4
+    return low, high, [((e + k) % experts, t) for k in range(1, experts)] + [(e, low), (e, high)]
+
+
+def dispatch_kernel(experts, send, kv, out, kv_out, *sems):
+    e, t = lax.axis_index("ep"), lax.axis_index("tp")
+    low, high, partners = all_partners(e, t, experts)
+    (a_send, a_recv, y_send, y_recv, l_send, l_recv, m_send, m_recv, k_send, k_recv, x_send, x_recv, own) = sems
+    half = experts // 2
+    side = e + 1 - 2 * (e % 2)
+
+    def remote(src, dst, s, r, device):
+        return pltpu.make_async_remote_copy(
+            src_ref=src, dst_ref=dst, send_sem=s, recv_sem=r, device_id=device, device_id_type=MESH
+        )
+
+    def kv_direct(k):
+        return remote(kv, kv_out.at[e], k_send.at[k], k_recv.at[k], ((e + 2 * k) % experts, t))
+
+    def kv_side(k):
+        owner = (e - 2 * k + experts) % experts
+        return remote(kv_out.at[owner], kv_out.at[owner], x_send.at[k], x_recv.at[k], (side, t))
+
+    def chunk(k):
+        return remote(send.at[(e + k) % experts], out.at[t, e], a_send.at[k], a_recv.at[k], ((e + k) % experts, t))
+
+    def source(k):
+        return (e - k + experts) % experts
+
+    def across(k):
+        block = out.at[t, source(k)]
+        return remote(block, block, y_send.at[k], y_recv.at[k], (e, high))
+
+    def beside(k):
+        block = out.at[t, source(k)]
+        return remote(block, block, l_send.at[k], l_recv.at[k], (e, low))
+
+    def relay(k):
+        block = out.at[high, source(k)]
+        return remote(block, block, m_send.at[k], m_recv.at[k], (e, low))
+
+    greet(partners)
+    own_chunk = pltpu.make_async_copy(send.at[e], out.at[t, e], own.at[0])
+    own_chunk.start()
+    own_kv = pltpu.make_async_copy(kv, kv_out.at[e], own.at[1])
+    own_kv.start()
+    lax.fori_loop(1, half, lambda k, c: (kv_direct(k).start(), c)[1], 0)
+    lax.fori_loop(1, experts, lambda k, c: (chunk(k).start(), c)[1], 0)
+    own_chunk.wait()
+    own_kv.wait()
+    across(0).start()
+    beside(0).start()
+    kv_side(0).start()
+
+    def step(k, carry):
+        chunk(k).wait_recv()
+        across(k).start()
+        beside(k).start()
+
+        @pl.when(k < half)
+        def _():
+            kv_direct(k).wait_recv()
+            kv_side(k).start()
+
+        @pl.when(k >= 2)
+        def _():
+            across(k - 2).wait_recv()
+            relay(k - 2).start()
+
+        return carry
+
+    lax.fori_loop(1, experts, step, 0)
+    for k in range(experts - 2, experts):
+        across(k).wait_recv()
+        relay(k).start()
+
+    def finish(k, carry):
+        across(k).wait_send()
+        beside(k).wait()
+        relay(k).wait()
+
+        @pl.when(k >= 1)
+        def _():
+            chunk(k).wait_send()
+
+        @pl.when(k < half)
+        def _():
+            kv_side(k).wait()
+
+        @pl.when((k >= 1) & (k < half))
+        def _():
+            kv_direct(k).wait_send()
+
+        return carry
+
+    lax.fori_loop(0, experts, finish, 0)
+
+
+def exchange(experts, send, kv):
+    vmem = pl.BlockSpec(memory_space=pltpu.VMEM)
+    sem = pltpu.SemaphoreType.DMA((experts,))
+    return pl.pallas_call(
+        functools.partial(dispatch_kernel, experts),
+        out_shape=(
+            jax.ShapeDtypeStruct((4,) + send.shape, send.dtype),
+            jax.ShapeDtypeStruct((experts,) + kv.shape, kv.dtype),
+        ),
+        in_specs=[vmem, vmem],
+        out_specs=(vmem, vmem),
+        scratch_shapes=[sem] * 12 + [pltpu.SemaphoreType.DMA((2,))],
+        name="dispatch",
+        compiler_params=pltpu.CompilerParams(
+            collective_id=1, has_side_effects=True, vmem_limit_bytes=58 * 2**20
+        ),
+    )(send, kv)
+
+
+def collect_kernel(experts, part, prod, ret, att, pair, pair_att, gone, gone_att, seen, seen_att, done, *sems):
+    e, t = lax.axis_index("ep"), lax.axis_index("tp")
+    low, high, partners = all_partners(e, t, experts)
+    low_high = (low + 2) % 4
+    (p_send, p_recv, q_send, q_recv, y_send, y_recv, a_send, a_recv, o_send, o_recv, own) = sems
+    middle = experts // 2
+
+    def remote(src, dst, s, r, device):
+        return pltpu.make_async_remote_copy(
+            src_ref=src, dst_ref=dst, send_sem=s, recv_sem=r, device_id=device, device_id_type=MESH
+        )
+
+    def target(k):
+        return (e + middle + k) % experts
+
+    def pair_far(k):
+        return remote(part.at[low_high, target(k)], pair.at[1, k], p_send.at[k], p_recv.at[k], (e, low))
+
+    def pair_near(k):
+        return remote(part.at[low, target(k)], pair.at[0, k], q_send.at[k], q_recv.at[k], (e, low))
+
+    def across(k):
+        return remote(gone.at[k], seen.at[k], y_send.at[k], y_recv.at[k], (e, high))
+
+    def back(k):
+        return remote(done.at[k], ret.at[e], a_send.at[k], a_recv.at[k], (target(k), t))
+
+    def other(i):
+        if i < 2:
+            return remote(prod.at[(low, low_high)[i]], pair_att.at[i], o_send.at[i], o_recv.at[i], (e, low))
+        return remote(gone_att, seen_att, o_send.at[i], o_recv.at[i], (e, high))
+
+    def local():
+        return pltpu.make_async_copy(done.at[middle], ret.at[e], own.at[0])
+
+    def deliver(k):
+        @pl.when(k == middle)
+        def _():
+            local().start()
+
+        @pl.when(k != middle)
+        def _():
+            back(k).start()
+
+    f32 = jnp.float32
+    greet(partners)
+    lax.fori_loop(0, experts, lambda k, c: (pair_far(k).start(), c)[1], 0)
+    other(1).start()
+    lax.fori_loop(0, experts, lambda k, c: (pair_near(k).start(), c)[1], 0)
+    other(0).start()
+
+    def first(k, carry):
+        pair_far(k).wait_recv()
+        gone[k] = (part[high, target(k)].astype(f32) + pair[1, k].astype(f32)).astype(gone.dtype)
+
+        @pl.when(k >= 1)
+        def _():
+            across(k - 1).start()
+
+        return carry
+
+    lax.fori_loop(0, experts, first, 0)
+    other(1).wait_recv()
+    gone_att[...] = (prod[high].astype(f32) + pair_att[1].astype(f32)).astype(gone_att.dtype)
+    across(experts - 1).start()
+
+    def second(k, carry):
+        pair_near(k).wait_recv()
+        across(k).wait_recv()
+
+        @pl.when(k == 0)
+        def _():
+            other(2).start()
+
+        total = part[t, target(k)].astype(f32) + pair[0, k].astype(f32) + seen[k].astype(f32)
+        done[k] = total.astype(done.dtype)
+
+        @pl.when(k >= 1)
+        def _():
+            deliver(k - 1)
+
+        return carry
+
+    lax.fori_loop(0, experts, second, 0)
+    other(0).wait_recv()
+    deliver(experts - 1)
+    other(2).wait_recv()
+    att[...] = (prod[t].astype(f32) + pair_att[0].astype(f32) + seen_att[...].astype(f32)).astype(att.dtype)
+
+    def finish(k, carry):
+        pair_far(k).wait_send()
+        pair_near(k).wait_send()
+        across(k).wait_send()
+
+        @pl.when(k == middle)
+        def _():
+            local().wait()
+
+        @pl.when(k != middle)
+        def _():
+            back(k).wait()
+
+        return carry
+
+    lax.fori_loop(0, experts, finish, 0)
+    for i in range(3):
+        other(i).wait_send()
+
+
+def collect(experts, part, prod):
+    vmem = pl.BlockSpec(memory_space=pltpu.VMEM)
+    sem = pltpu.SemaphoreType.DMA((experts,))
+    row, att = part.shape[1:], prod.shape[1:]
+    like = part.dtype
+    return pl.pallas_call(
+        functools.partial(collect_kernel, experts),
+        out_shape=(jax.ShapeDtypeStruct(row, like), jax.ShapeDtypeStruct(att, like)),
+        in_specs=[vmem, vmem],
+        out_specs=(vmem, vmem),
+        scratch_shapes=[
+            pltpu.VMEM((2,) + row, like),
+            pltpu.VMEM((2,) + att, like),
+            pltpu.VMEM(row, like),
+            pltpu.VMEM(att, like),
+            pltpu.VMEM(row, like),
+            pltpu.VMEM(att, like),
+            pltpu.VMEM(row, like),
+        ]
+        + [sem] * 8
+        + [pltpu.SemaphoreType.DMA((3,))] * 2
+        + [pltpu.SemaphoreType.DMA((1,))],
+        name="collect",
+        compiler_params=pltpu.CompilerParams(
+            collective_id=2, has_side_effects=True, vmem_limit_bytes=58 * 2**20
+        ),
+    )(part, prod)
 
 
 def per_device(
@@ -59,14 +328,44 @@
     value_heads = values.reshape(pos_count, seq_count, kv_local, HEAD_DIM)
     q_group = q_rot.reshape(pos_count, seq_count, kv_local, groups, HEAD_DIM)
     scale = HEAD_DIM ** (-0.5)
+    tok_count = moe_tokens.shape[0]
+    top_count = routes.shape[1]
+    experts = lax.axis_size("ep")
+    capacity = max(2, (3 * tok_count * top_count + 2 * experts - 1) // (2 * experts))
+    token_float = moe_tokens.astype(jnp.float32)
+    normed = (
+        token_float
+        * lax.rsqrt(jnp.mean(token_float * token_float, axis=-1, keepdims=True) + EPS)
+        * moe_gain
+    ).astype(jnp.bfloat16)
+    hits = (routes[:, :, None] == jnp.arange(experts, dtype=jnp.int32)[None, None, :]).astype(
+        jnp.float32
+    )
+    pair_count = tok_count * top_count
+    flat_hits = hits.reshape(pair_count, experts)
+    pair_index = jnp.arange(pair_count, dtype=jnp.int32)
+    earlier = (pair_index[:, None] > pair_index[None, :]).astype(jnp.float32)
+    before = jnp.dot(earlier, flat_hits, precision=lax.Precision.HIGHEST)
+    rank = jnp.sum(before * flat_hits, axis=-1).astype(jnp.int32).reshape(tok_count, top_count)
+    slot = routes * capacity + rank
+    table = jnp.arange(experts * capacity, dtype=jnp.int32)
+    dispatch = jnp.sum(
+        (slot[None, :, :] == table[:, None, None]).astype(jnp.float32), axis=2
+    ).astype(jnp.bfloat16)
+    send = jnp.dot(dispatch, normed, preferred_element_type=jnp.float32).astype(jnp.bfloat16)
     start_state = (
         jnp.full((seq_count, kv_local, groups, pos_count), -1e30, jnp.float32),
         jnp.zeros((seq_count, kv_local, groups, pos_count), jnp.float32),
         jnp.zeros((pos_count, seq_count, kv_local, groups, HEAD_DIM), jnp.float32),
     )
     carry = start_state
-    key_piece = lax.all_gather(k_rot, "ep", axis=0, tiled=True)
-    value_piece = lax.all_gather(value_heads, "ep", axis=0, tiled=True)
+    kv = jnp.concatenate([k_rot, value_heads], axis=-1)
+    kv = jnp.transpose(kv, (1, 2, 0, 3)).reshape(seq_count * kv_local * pos_count, 2 * HEAD_DIM)
+    rows, kv_all = exchange(experts, send.reshape(experts, capacity, -1), kv)
+    kv_all = kv_all.reshape(experts, seq_count, kv_local, pos_count, 2 * HEAD_DIM)
+    kv_all = jnp.transpose(kv_all, (0, 3, 1, 2, 4)).reshape(experts * pos_count, seq_count, kv_local, 2 * HEAD_DIM)
+    key_piece = kv_all[..., :HEAD_DIM]
+    value_piece = kv_all[..., HEAD_DIM:]
     count = key_piece.shape[0]
     width = math.gcd(count, 512)
     key_split = key_piece.reshape(count // width, width, seq_count, kv_local, HEAD_DIM)
@@ -96,58 +395,24 @@
     best, total, accum = carry
     mixed = (accum / jnp.transpose(total, (3, 0, 1, 2))[..., None]).astype(jnp.bfloat16)
     mixed = mixed.reshape(pos_count, seq_count, -1)
-    rows = mixed
     product = jnp.dot(
-        rows.reshape(pos_count // lax.axis_size("tp") * lax.axis_size("tp") * seq_count, -1),
+        mixed.reshape(pos_count * seq_count, -1),
         out_weight,
         preferred_element_type=jnp.float32,
     )
-    attended = lax.psum_scatter(
-        product.reshape(
-            pos_count // lax.axis_size("tp") * lax.axis_size("tp"), seq_count, -1
-        ).astype(jnp.bfloat16),
-        "tp",
-        scatter_dimension=0,
-        tiled=True,
-    )
-    tok_count = moe_tokens.shape[0]
-    top_count = routes.shape[1]
-    experts = lax.axis_size("ep")
-    capacity = max(2, (3 * tok_count * top_count + 2 * experts - 1) // (2 * experts))
-    token_float = moe_tokens.astype(jnp.float32)
-    normed = (
-        token_float
-        * lax.rsqrt(jnp.mean(token_float * token_float, axis=-1, keepdims=True) + EPS)
-        * moe_gain
-    ).astype(jnp.bfloat16)
-    hits = (routes[:, :, None] == jnp.arange(experts, dtype=jnp.int32)[None, None, :]).astype(
-        jnp.float32
-    )
-    pair_count = tok_count * top_count
-    flat_hits = hits.reshape(pair_count, experts)
-    pair_index = jnp.arange(pair_count, dtype=jnp.int32)
-    earlier = (pair_index[:, None] > pair_index[None, :]).astype(jnp.float32)
-    before = jnp.dot(earlier, flat_hits, precision=lax.Precision.HIGHEST)
-    rank = jnp.sum(before * flat_hits, axis=-1).astype(jnp.int32).reshape(tok_count, top_count)
-    slot = routes * capacity + rank
-    table = jnp.arange(experts * capacity, dtype=jnp.int32)
-    dispatch = jnp.sum(
-        (slot[None, :, :] == table[:, None, None]).astype(jnp.float32), axis=2
-    ).astype(jnp.bfloat16)
-    send = jnp.dot(dispatch, normed, preferred_element_type=jnp.float32).astype(jnp.bfloat16)
-    received = lax.all_to_all(send, "ep", split_axis=0, concat_axis=0, tiled=True)
-    rows = lax.all_gather(received, "tp", axis=0, tiled=True)
-    gate = jnp.dot(rows, w_gate[0], preferred_element_type=jnp.float32)
-    up = jnp.dot(rows, w_up[0], preferred_element_type=jnp.float32)
+    tp = lax.axis_size("tp")
+    gathered = rows.reshape(tp * experts * capacity, -1)
+    gate = jnp.dot(gathered, w_gate[0], preferred_element_type=jnp.float32)
+    up = jnp.dot(gathered, w_up[0], preferred_element_type=jnp.float32)
     hidden = (jax.nn.silu(gate) * up).astype(jnp.bfloat16)
-    rows = hidden
-    result = lax.psum_scatter(
-        jnp.dot(rows, w_down[0], preferred_element_type=jnp.float32).astype(jnp.bfloat16),
-        "tp",
-        scatter_dimension=0,
-        tiled=True,
-    )
-    returned_rows = lax.all_to_all(result, "ep", split_axis=0, concat_axis=0, tiled=True)
+    part = jnp.dot(hidden, w_down[0], preferred_element_type=jnp.float32).astype(jnp.bfloat16)
+    returned_rows, attended = collect(
+        experts,
+        part.reshape(tp, experts, capacity, -1),
+        product.astype(jnp.bfloat16).reshape(tp, pos_count // tp * seq_count, -1),
+    )
+    returned_rows = returned_rows.reshape(experts * capacity, -1)
+    attended = attended.reshape(pos_count // tp, seq_count, -1)
     combined = jnp.zeros((tok_count, returned_rows.shape[-1]), jnp.float32)
     for choice_index in range(top_count):
         picker = (slot[:, choice_index : choice_index + 1] == table[None, :]).astype(jnp.bfloat16)

time: 242 us -> 196 us (0.81)
  Pallas kernels: 0 us -> 136 us
  blocking collectives: 107 us -> 0 us
  waiting for transfers between devices: 71.3 us -> 0 us
  between operations: 14 us -> 0.89 us
  local copies, waits for them, and re-layouts: 5.07 us -> 12.8 us
  starting transfers between devices: 5.78 us -> 0 us
  matrix products: 31.9 us -> 36.3 us
  other arithmetic: 5.82 us -> 8.37 us
    pallas_call x0 -> x2, Pallas kernels: none -> 136 us  [the longest x1 69.2 us: exchange(): pl.pallas_call(functools.partial(dispatch_kernel, experts), out_shape=(ja...]
    all_gather x2 -> x0, blocking collectives: 62.9 us -> none  [the longest x1 31.5 us: per_device(): value_piece = lax.all_gather(value_heads, 'ep', axis=0, tiled=True)]
    all_gather x1 -> x0, waiting for transfers between devices: 45.5 us -> none  [per_device(): rows = lax.all_gather(received, 'tp', axis=0, tiled=True)]
    all_to_all x1 -> x0, blocking collectives: 44.2 us -> none  [per_device(): lax.all_to_all(send, 'ep', split_axis=0, concat_axis=0, tiled=True)]
    reduce_scatter x2 -> x0, waiting for transfers between devices: 25.8 us -> none  [the longest x1 25.8 us: per_device(): lax.psum_scatter(product.reshape(pos_count // lax.axis_size('tp') * lax.a...]
    all_to_all x1 -> x0, starting transfers between devices: 5.66 us -> none  [per_device(): lax.all_to_all(result, 'ep', split_axis=0, concat_axis=0, tiled=True)]
    dot_general x4, matrix products: 3.08 us -> 6.75 us  [step(): jnp.einsum('pskgd,lskd->skgpl', q_group, key_block, preferred_element_typ...]
    reshape x2, local copies, waits for them, and re-layouts: 0.42 us -> 3.59 us  [the longest x1 2.29 us: per_device(): attended = attended.reshape(pos_count // tp, seq_count, -1)]
  transfers between devices with their start and end apart: 4 -> 0, of which waited for: 2 -> 0; matrix products, arithmetic and copies ran while one was open for 7% -> 0% of each run, Pallas kernels for 0% -> 0%
where the time goes in v1:
time: 196 us; the launch traced here: 195 us
  Pallas kernels  136 us (69%)
  matrix products  36.3 us (19%)
  local copies, waits for them, and re-layouts  12.8 us (7%)
  other arithmetic  8.37 us (4%)
    pallas_call x1, Pallas kernels, exchange(): pl.pallas_call(functools.partial(dispatch_kernel, experts), out_shape=(ja...  69.2 us
    pallas_call x1, Pallas kernels, collect(): pl.pallas_call(functools.partial(collect_kernel, experts), out_shape=(jax...  67.2 us
    dot_general x1, matrix products, per_device(): jnp.dot(hidden, w_down[0], preferred_element_type=jnp.float32)  12.7 us
    dot_general x4, matrix products, step(): jnp.einsum('pskgd,lskd->skgpl', q_group, key_block, preferred_element_typ...  6.75 us
    dot_general x1, matrix products, per_device(): gate = jnp.dot(gathered, w_gate[0], preferred_element_type=jnp.float32)  5.79 us
    unnamed x16, local copies, waits for them, and re-layouts  4.6 us

profile of v1, /device:TPU:0, one launch (start us, length us, event | category | flops | bytes accessed | tf_op | source)
XLA Modules:
  0.0 195.1 jit_solution(10494456260345274346)
XLA Ops:
  0.7 1.3 fusion.28
  2.0 0.8 slice_bitcast_fusion
  2.8 0.7 mul.285
  3.6 0.9 fusion.40
  4.7 0.8 copy.57
  6.8 0.9 fusion.41
  7.7 0.9 maximum_bitcast_fusion
  8.6 0.8 copy.59
  9.4 1.1 copy.62
  10.8 1.8 convolution_convert_fusion.2
  12.6 69.2 %dispatch.1 = (bf16[4,8,48,2048]{3,2,1,0:T(8,128)(2,1)}, bf16[8,512,128]{2,1,0:T(8,128)(2,1)}) custom-call(bf16[8,48,2048]{2,1,0:T(8,128)(2,1)} %bitcast.141, bf16[512,128]{1,0:T(8,128)(2,1)} %bitcast.150), custom_call_target="tpu_custom_call" | custom-call | tf_op jit(solution)/shard_map/dispatch/pallas_call | solution.py:152
  81.8 1.3 copy.60
  83.1 1.4 fusion.52
  84.5 1.5 copy.65
  86.1 1.1 copy.64
  87.2 13.9 %while.15 = (s32[]{:T(128)}, f32[2,1,4,256]{3,2,0,1:T(4,128)S(1)}, f32[2,1,4,256]{3,2,0,1:T(4,128)S(1)}, f32[256,2,1,4,64]{0,4,3,1,2:T(8,128)S(1)}, bf16[4,512,2...) while((s32[]{:T(128)}, f32[2,1,4,256]{3,2,0,1:T(4,128)S(1)}, ...), condition=%wide.region_8.9_spmd.clone, body=%wide.region_5.8_spmd.clone.sunk | while | flops 277229568 | bytes 14286969 | solution.py:394
  87.2 1.8 bitcast_reduce_fusion.3
  89.7 1.0 fusion.69
  90.7 1.7 bitcast_reduce_fusion.3
  93.1 1.0 fusion.69
  94.1 1.7 bitcast_reduce_fusion.3
  95.8 0.7 fusion.68
  96.5 1.0 fusion.69
  97.5 1.7 bitcast_reduce_fusion.3
  99.9 1.0 fusion.69
  101.9 5.8 %fusion.34 = f32[1536,256]{1,0:T(8,128)} fusion(bf16[1536,2048]{1,0:T(8,128)(2,1)} %bitcast.154, bf16[1,2048,256]{2,1,0:T(8,128)(2,1)S(1)} %copy-done.5), kind=kOutput, calls=%fused_computation.44 | convolution fusion | flops 1610612736 | bytes 8912896 | tf_op jit(solution)/shard_map/dot_general | solution.py:405
  107.7 12.7 %convolution_convert_fusion = bf16[1536,2048]{1,0:T(8,128)(2,1)} fusion(bf16[1536,2048]{1,0:T(8,128)(2,1)} %bitcast.155, f32[1536,256]{1,0:T(8,128)} %fusion.34, bf16[1,256,2048]{2,1,0:T(8,128)(2,1)S(1)} %copy-done, bf16[1,2048,256]{2,1,0:T(8,128)(2,1)} %param.26), kind=kOutput, calls=%fused_computation.26 | convolution fusion | flops 3226730496 | bytes 16252928 | tf_op jit(solution)/shard_map/dot_general | solution.py:408
  120.3 2.1 %convolution_convert_fusion.1 = bf16[512,2048]{1,0:T(8,128)(2,1)} fusion(bf16[512,256]{1,0:T(8,128)(2,1)S(1)} %reshape_reshape.3, bf16[256,2048]{1,0:T(8,128)(2,1)S(1)} %copy-done.3), kind=kOutput, calls=%fused_computation.27 | convolution fusion | flops 537919488 | bytes 3407872 | tf_op jit(solution)/shard_map/dot_general | solution.py:398
  122.4 67.2 %collect.1 = (bf16[8,48,2048]{2,1,0:T(8,128)(2,1)}, bf16[128,2048]{1,0:T(8,128)(2,1)}) custom-call(bf16[4,8,48,2048]{3,2,1,0:T(8,128)(2,1)} %bitcast.142, bf16[4,128,2048]{2,1,0:T(8,128)(2,1)} %bitcast.138), custom_call_target="tpu_custom_call" | custom-call | tf_op jit(solution)/shard_map/collect/pallas_call | solution.py:282
  189.6 2.3 %reshape.317 = bf16[64,2,2048]{2,1,0:T(2,128)(2,1)} reshape(bf16[128,2048]{1,0:T(8,128)(2,1)} %get-tuple-element.48) | data formatting | bytes 1048576 | tf_op jit(solution)/shard_map/reshape | solution.py:415
  191.9 1.9 convolution_multiply_fusion.2
  193.8 1.3 fusion.26
  (54 shorter events, 4.9 us)
Async XLA Ops:
  0.6 107.0 %copy-start = (bf16[1,256,2048]{2,1,0:T(8,128)(2,1)S(1)}, bf16[1,256,2048]{2,1,0:T(8,128)(2,1)}, u32[]{:S(2)}) copy-start(bf16[1,256,2048]{2,1,0:T(8,128)(2,1)} %param.27) | copy-start | bytes 3145732
  0.6 10.2 %copy-start.2 = (bf16[128,2048]{1,0:T(8,128)(2,1)S(1)}, bf16[128,2048]{1,0:T(8,128)(2,1)}, u32[]{:S(2)}) copy-start(bf16[128,2048]{1,0:T(8,128)(2,1)} %param.21) | copy-start | bytes 1572868
  0.7 10.2 %copy-start.4 = (f32[2048]{0:T(1024)S(1)}, f32[2048]{0:T(1024)}, u32[]{:S(2)}) copy-start(f32[2048]{0:T(1024)} %param.22) | copy-start | bytes 24580
  87.2 14.7 %copy-start.5 = (bf16[1,2048,256]{2,1,0:T(8,128)(2,1)S(1)}, bf16[1,2048,256]{2,1,0:T(8,128)(2,1)}, u32[]{:S(2)}) copy-start(bf16[1,2048,256]{2,1,0:T(8,128)(2,1)} %param.25) | copy-start | bytes 3145732
  107.7 12.7 %copy-start.3 = (bf16[256,2048]{1,0:T(8,128)(2,1)S(1)}, bf16[256,2048]{1,0:T(8,128)(2,1)}, u32[]{:S(2)}) copy-start(bf16[256,2048]{1,0:T(8,128)(2,1)} %param.20) | copy-start | bytes 3145732
  189.6 4.2 %copy-start.1 = (bf16[8,48,2048]{2,1,0:T(8,128)(2,1)S(1)}, bf16[8,48,2048]{2,1,0:T(8,128)(2,1)}, u32[]{:S(2)}) copy-start(bf16[8,48,2048]{2,1,0:T(8,128)(2,1)} %get-tuple-element.49) | copy-start | bytes 4718596

commit v2 on v0

v2 whole, which is shorter than its diff:
```python
import functools

import jax
import jax.numpy as jnp
from jax import lax
from jax.experimental import pallas as pl
from jax.experimental.pallas import tpu as pltpu
from jax.sharding import PartitionSpec as P

HEAD_DIM = 64
GRID_W = 64


EPS = 1e-06
THETA = 10000.0


def turn(normed, positions):
    quarter = normed.shape[-1] // 4
    inverse = THETA ** (-jnp.arange(quarter, dtype=jnp.float32) / quarter)
    grid_row = (positions // GRID_W).astype(jnp.float32)
    grid_col = (positions % GRID_W).astype(jnp.float32)
    angles = jnp.stack([grid_row[:, None] * inverse, grid_col[:, None] * inverse], axis=1)
    cosine = jnp.cos(angles)[:, None, None]
    sine = jnp.sin(angles)[:, None, None]
    parts = normed.reshape(normed.shape[:-1] + (2, 2, quarter))
    first = parts[..., 0, :]
    second = parts[..., 1, :]
    turned = jnp.stack([first * cosine - second * sine, second * cosine + first * sine], axis=-2)
    return turned.reshape(normed.shape)


def prepare(data, positions, gain):
    heads = data.astype(jnp.float32).reshape(data.shape[0], data.shape[1], -1, HEAD_DIM)
    normed = heads * lax.rsqrt(jnp.mean(heads * heads, axis=-1, keepdims=True) + EPS) * gain
    return turn(normed, positions).astype(jnp.bfloat16)


MESH = pl.DeviceIdType.MESH


def fused_kernel(experts, send, kv, q, out_weight, w_gate, w_up, w_down, ret, att, *scratch):
    (rows, kv_all, part, pair, gone, seen, done, prod, pair_att, gone_att, seen_att, packed, accum, best, total) = scratch[:15]
    (a_send, a_recv, y_send, y_recv, l_send, l_recv, m_send, m_recv, k_send, k_recv, x_send, x_recv) = scratch[15:27]
    (f_send, f_recv, n_send, n_recv, c_send, c_recv, b_send, b_recv, o_send, o_recv, own) = scratch[27:]
    f32, bf16 = jnp.float32, jnp.bfloat16
    e, t = lax.axis_index("ep"), lax.axis_index("tp")
    low, high = t + 1 - 2 * (t % 2), (t + 2) % 4
    low_high = (low + 2) % 4
    half = experts // 2
    side = e + 1 - 2 * (e % 2)
    capacity = send.shape[1]
    stride = packed.shape[0] // 4

    def remote(src, dst, s, r, device):
        return pltpu.make_async_remote_copy(
            src_ref=src, dst_ref=dst, send_sem=s, recv_sem=r, device_id=device, device_id_type=MESH
        )

    def source(k):
        return (e - k + experts) % experts

    def kv_direct(k):
        return remote(kv, kv_all.at[e], k_send.at[k], k_recv.at[k], ((e + 2 * k) % experts, t))

    def kv_side(k):
        block = kv_all.at[(e - 2 * k + experts) % experts]
        return remote(block, block, x_send.at[k], x_recv.at[k], (side, t))

    def chunk(k):
        return remote(send.at[(e + k) % experts], rows.at[t, e], a_send.at[k], a_recv.at[k], ((e + k) % experts, t))

    def across(k):
        block = rows.at[t, source(k)]
        return remote(block, block, y_send.at[k], y_recv.at[k], (e, high))

    def beside(k):
        block = rows.at[t, source(k)]
        return remote(block, block, l_send.at[k], l_recv.at[k], (e, low))

    def relay(k):
        block = rows.at[high, source(k)]
        return remote(block, block, m_send.at[k], m_recv.at[k], (e, low))

    def pair_far(k):
        return remote(part.at[low_high, k], pair.at[1, k], f_send.at[k], f_recv.at[k], (e, low))

    def pair_near(k):
        return remote(part.at[low, k], pair.at[0, k], n_send.at[k], n_recv.at[k], (e, low))

    def over(k):
        return remote(gone.at[k], seen.at[k], c_send.at[k], c_recv.at[k], (e, high))

    def back(k):
        return remote(done.at[k], ret.at[e], b_send.at[k], b_recv.at[k], (source(k), t))

    def other(i):
        if i < 2:
            return remote(prod.at[(low, low_high)[i]], pair_att.at[i], o_send.at[i], o_recv.at[i], (e, low))
        return remote(gone_att, seen_att, o_send.at[i], o_recv.at[i], (e, high))

    def attend(owner):
        for s in range(kv.shape[0]):
            block = kv_all[owner, s]
            scores = lax.dot_general(block, q[s], (((1,), (1,)), ((), ())), preferred_element_type=f32)
            old = best[s]
            new = jnp.maximum(old, jnp.max(scores, axis=0, keepdims=True))
            factor = jnp.exp(old - new)
            expo = jnp.exp(scores - new)
            best[s] = new
            total[s] = total[s] * factor + jnp.sum(expo, axis=0, keepdims=True)
            added = lax.dot_general(block, expo.astype(bf16), (((0,), (0,)), ((), ())), preferred_element_type=f32)
            accum[s] = accum[s] * factor + added

    def project():
        positions = kv.shape[1]
        quarter = positions // 4
        for s in range(kv.shape[0]):
            mixed = (accum[s, HEAD_DIM:, :] / total[s]).astype(bf16)
            groups = mixed.shape[1] // positions
            stacked = jnp.concatenate([mixed[:, g * positions : (g + 1) * positions] for g in range(groups)], axis=0)
            product = lax.dot_general(stacked, out_weight[...], (((0,), (0,)), ((), ())), preferred_element_type=f32)
            product = product.astype(bf16)
            for b in range(4):
                prod[b, s * quarter : (s + 1) * quarter, :] = product[b * quarter : (b + 1) * quarter]

    def expert(k):
        for b in range(4):
            packed[b * stride : b * stride + capacity, :] = rows[b, source(k)]
        data = packed[...]
        gate = jnp.dot(data, w_gate[...], preferred_element_type=f32)
        up = jnp.dot(data, w_up[...], preferred_element_type=f32)
        hidden = (gate * (1.0 / (1.0 + jnp.exp(-gate))) * up).astype(bf16)
        result = jnp.dot(hidden, w_down[...], preferred_element_type=f32).astype(bf16)
        for b in range(4):
            part[b, k] = result[b * stride : b * stride + capacity]

    barrier = pltpu.get_barrier_semaphore()
    partners = [((e + k) % experts, t) for k in range(1, experts)] + [(e, low), (e, high)]
    for device in partners:
        pl.semaphore_signal(barrier, inc=1, device_id=device, device_id_type=MESH)
    pl.semaphore_wait(barrier, len(partners))

    own_chunk = pltpu.make_async_copy(send.at[e], rows.at[t, e], own.at[0])
    own_chunk.start()
    own_kv = pltpu.make_async_copy(kv, kv_all.at[e], own.at[1])
    own_kv.start()
    lax.fori_loop(1, half, lambda k, c: (kv_direct(k).start(), c)[1], 0)
    lax.fori_loop(1, experts, lambda k, c: (chunk(k).start(), c)[1], 0)
    best[...] = jnp.full_like(best, -1e30)
    total[...] = jnp.zeros_like(total)
    accum[...] = jnp.zeros_like(accum)
    own_chunk.wait()
    own_kv.wait()
    kv_side(0).start()

    def step(k, carry):
        @pl.when((k >= 1) & (k < experts))
        def _():
            chunk(k).wait_recv()

        @pl.when(k < experts)
        def _():
            across(k).start()
            beside(k).start()

        @pl.when((k >= 1) & (k < half))
        def _():
            kv_direct(k).wait_recv()
            kv_side(k).start()

        @pl.when((k >= half) & (k < experts))
        def _():
            kv_side(k - half).wait_recv()

        @pl.when(k < experts)
        def _():
            direct = (e - 2 * k + 2 * experts) % experts
            beyond = (side - 2 * (k - half) + 2 * experts) % experts
            near = (experts + half - 1 - k) // experts
            attend(near * direct + (1 - near) * beyond)

        @pl.when(k == experts)
        def _():
            project()

        @pl.when(k == experts + 1)
        def _():
            other(1).start()
            other(0).start()

        @pl.when((k >= 2) & (k < experts + 2))
        def _():
            across(k - 2).wait_recv()
            relay(k - 2).start()

        @pl.when((k >= 4) & (k < experts + 4))
        def _():
            pair_far(k - 4).start()
            pair_near(k - 4).start()

        @pl.when((k >= 3) & (k < experts + 3))
        def _():
            beside(k - 3).wait_recv()
            relay(k - 3).wait_recv()
            expert(k - 3)

        @pl.when((k >= 6) & (k < experts + 6))
        def _():
            over(k - 6).start()

        @pl.when((k >= 5) & (k < experts + 5))
        def _():
            j = k - 5
            pair_far(j).wait_recv()
            gone[j] = (part[high, j].astype(f32) + pair[1, j].astype(f32)).astype(bf16)

        @pl.when(k == experts + 6)
        def _():
            other(1).wait_recv()
            gone_att[...] = (prod[high].astype(f32) + pair_att[1].astype(f32)).astype(bf16)

        @pl.when(k == experts + 7)
        def _():
            other(2).start()

        @pl.when(k == 9)
        def _():
            pltpu.make_async_copy(done.at[0], ret.at[e], own.at[0]).start()

        @pl.when((k >= 10) & (k < experts + 9))
        def _():
            back(k - 9).start()

        @pl.when((k >= 8) & (k < experts + 8))
        def _():
            j = k - 8
            pair_near(j).wait_recv()
            over(j).wait_recv()
            done[j] = (part[t, j].astype(f32) + pair[0, j].astype(f32) + seen[j].astype(f32)).astype(bf16)

        return carry

    lax.fori_loop(0, experts + 9, step, 0)
    other(0).wait_recv()
    other(2).wait_recv()
    att[...] = (prod[t].astype(f32) + pair_att[0].astype(f32) + seen_att[...].astype(f32)).astype(bf16)

    def finish(k, carry):
        across(k).wait_send()
        beside(k).wait_send()
        relay(k).wait_send()
        pair_far(k).wait_send()
        pair_near(k).wait_send()
        over(k).wait_send()

        @pl.when(k >= 1)
        def _():
            chunk(k).wait_send()
            back(k).wait()

        @pl.when(k < half)
        def _():
            kv_side(k).wait_send()

        @pl.when((k >= 1) & (k < half))
        def _():
            kv_direct(k).wait_send()

        return carry

    lax.fori_loop(0, experts, finish, 0)
    for i in range(3):
        other(i).wait_send()
    pltpu.make_async_copy(done.at[0], ret.at[e], own.at[0]).wait()


def fused(experts, send, kv, q, out_weight, w_gate, w_up, w_down):
    sem = pltpu.SemaphoreType.DMA((experts,))
    like = send.dtype
    capacity, features = send.shape[1:]
    seqs, positions, lanes = kv.shape
    att = (positions // 4 * seqs, features)
    queries = q.shape[1]
    stride = -(-capacity // 16) * 16
    shapes = [
        (4,) + send.shape,
        (experts,) + kv.shape,
        (4,) + send.shape,
        (2,) + send.shape,
        send.shape,
        send.shape,
        send.shape,
        (4,) + att,
        (2,) + att,
        att,
        att,
        (4 * stride, features),
    ]
    vmem = pl.BlockSpec(memory_space=pltpu.VMEM)
    return pl.pallas_call(
        functools.partial(fused_kernel, experts),
        out_shape=(jax.ShapeDtypeStruct(send.shape, like), jax.ShapeDtypeStruct(att, like)),
        in_specs=[vmem] * 7,
        out_specs=(vmem, vmem),
        scratch_shapes=[pltpu.VMEM(shape, like) for shape in shapes]
        + [
            pltpu.VMEM((seqs, lanes, queries), jnp.float32),
            pltpu.VMEM((seqs, 1, queries), jnp.float32),
            pltpu.VMEM((seqs, 1, queries), jnp.float32),
        ]
        + [sem] * 20
        + [pltpu.SemaphoreType.DMA((3,))] * 2
        + [pltpu.SemaphoreType.DMA((2,))],
        name="fused",
        compiler_params=pltpu.CompilerParams(
            collective_id=1, has_side_effects=True, vmem_limit_bytes=62 * 2**20
        ),
    )(send, kv, q, out_weight, w_gate, w_up, w_down)


def per_device(
    queries,
    keys,
    values,
    query_gain,
    key_gain,
    out_weight,
    moe_tokens,
    moe_gain,
    routes,
    route_weight,
    w_gate,
    w_up,
    w_down,
):
    pos_count = queries.shape[0]
    seq_count = queries.shape[1]
    positions = lax.axis_index("ep") * pos_count + jnp.arange(pos_count, dtype=jnp.int32)
    q_rot = prepare(queries, positions, query_gain)
    k_rot = prepare(keys, positions, key_gain)
    kv_local = k_rot.shape[2]
    groups = q_rot.shape[2] // kv_local
    value_heads = values.reshape(pos_count, seq_count, kv_local, HEAD_DIM)
    q_group = q_rot.reshape(pos_count, seq_count, kv_local, groups, HEAD_DIM)
    scale = HEAD_DIM ** (-0.5)
    tok_count = moe_tokens.shape[0]
    top_count = routes.shape[1]
    experts = lax.axis_size("ep")
    capacity = max(2, (3 * tok_count * top_count + 2 * experts - 1) // (2 * experts))
    token_float = moe_tokens.astype(jnp.float32)
    normed = (
        token_float
        * lax.rsqrt(jnp.mean(token_float * token_float, axis=-1, keepdims=True) + EPS)
        * moe_gain
    ).astype(jnp.bfloat16)
    hits = (routes[:, :, None] == jnp.arange(experts, dtype=jnp.int32)[None, None, :]).astype(
        jnp.float32
    )
    pair_count = tok_count * top_count
    flat_hits = hits.reshape(pair_count, experts)
    pair_index = jnp.arange(pair_count, dtype=jnp.int32)
    earlier = (pair_index[:, None] > pair_index[None, :]).astype(jnp.float32)
    before = jnp.dot(earlier, flat_hits, precision=lax.Precision.HIGHEST)
    rank = jnp.sum(before * flat_hits, axis=-1).astype(jnp.int32).reshape(tok_count, top_count)
    slot = routes * capacity + rank
    table = jnp.arange(experts * capacity, dtype=jnp.int32)
    dispatch = jnp.sum(
        (slot[None, :, :] == table[:, None, None]).astype(jnp.float32), axis=2
    ).astype(jnp.bfloat16)
    send = jnp.dot(dispatch, normed, preferred_element_type=jnp.float32).astype(jnp.bfloat16)
    kv = jnp.concatenate([k_rot, value_heads], axis=-1)
    kv = jnp.transpose(kv, (1, 2, 0, 3)).reshape(seq_count * kv_local, pos_count, 2 * HEAD_DIM)
    q_rows = jnp.transpose(q_group * jnp.bfloat16(scale), (1, 2, 3, 0, 4))
    q_rows = jnp.pad(q_rows, ((0, 0),) * 4 + ((0, HEAD_DIM),))
    q_rows = q_rows.reshape(seq_count * kv_local, groups * pos_count, 2 * HEAD_DIM)
    returned_rows, attended = fused(
        experts,
        send.reshape(experts, capacity, -1),
        kv,
        q_rows,
        out_weight,
        w_gate[0],
        w_up[0],
        w_down[0],
    )
    returned_rows = returned_rows.reshape(experts * capacity, -1)
    quarter = pos_count // lax.axis_size("tp")
    attended = jnp.transpose(attended.reshape(seq_count, quarter, -1), (1, 0, 2))
    combined = jnp.zeros((tok_count, returned_rows.shape[-1]), jnp.float32)
    for choice_index in range(top_count):
        picker = (slot[:, choice_index : choice_index + 1] == table[None, :]).astype(jnp.bfloat16)
        picked = jnp.dot(picker, returned_rows, preferred_element_type=jnp.float32)
        combined = combined + picked * route_weight[:, choice_index : choice_index + 1]
    return (attended, combined.astype(jnp.bfloat16))


def solution(mesh):
    in_specs = (
        P("ep", None, "tp"),
        P("ep", None, "tp"),
        P("ep", None, "tp"),
        P(),
        P(),
        P("tp", None),
        P(("ep", "tp"), None),
        P(),
        P(("ep", "tp"), None),
        P(("ep", "tp"), None),
        P("ep", None, "tp"),
        P("ep", None, "tp"),
        P("ep", "tp", None),
    )
    out_specs = (P(("ep", "tp"), None, None), P(("ep", "tp"), None))
    return jax.shard_map(
        per_device, mesh=mesh, in_specs=in_specs, out_specs=out_specs, check_vma=False
    )
```

time: 242 us -> 140 us (0.58)
  Pallas kernels: 0 us -> 126 us
  blocking collectives: 107 us -> 0 us
  waiting for transfers between devices: 71.3 us -> 0 us
  matrix products: 31.9 us -> 5.33 us
  between operations: 14 us -> 0.89 us
  starting transfers between devices: 5.78 us -> 0 us
  other arithmetic: 5.82 us -> 1.74 us
    pallas_call x0 -> x1, Pallas kernels: none -> 126 us  [fused(): pl.pallas_call(functools.partial(fused_kernel, experts), out_shape=(jax.S...]
    all_gather x2 -> x0, blocking collectives: 62.9 us -> none  [the longest x1 31.5 us: per_device(): value_piece = lax.all_gather(value_heads, 'ep', axis=0, tiled=True)]
    all_gather x1 -> x0, waiting for transfers between devices: 45.5 us -> none  [per_device(): rows = lax.all_gather(received, 'tp', axis=0, tiled=True)]
    all_to_all x1 -> x0, blocking collectives: 44.2 us -> none  [per_device(): lax.all_to_all(send, 'ep', split_axis=0, concat_axis=0, tiled=True)]
    dot_general x11 -> x0, matrix products: 28.3 us -> none  [the longest x1 12.3 us: per_device(): jnp.dot(rows, w_down[0], preferred_element_type=jnp.float32)]
    reduce_scatter x2 -> x0, waiting for transfers between devices: 25.8 us -> none  [the longest x1 25.8 us: per_device(): lax.psum_scatter(product.reshape(pos_count // lax.axis_size('tp') * lax.a...]
    all_to_all x1 -> x0, starting transfers between devices: 5.66 us -> none  [per_device(): lax.all_to_all(result, 'ep', split_axis=0, concat_axis=0, tiled=True)]
    reduce_sum x4 -> x0, other arithmetic: 2.82 us -> none  [step(): total = total * factor + jnp.sum(expo, axis=-1)]
  transfers between devices with their start and end apart: 4 -> 0, of which waited for: 2 -> 0; matrix products, arithmetic and copies ran while one was open for 7% -> 0% of each run, Pallas kernels for 0% -> 0%
where the time goes in v2:
time: 140 us; the launch traced here: 139 us
  Pallas kernels  126 us (90%)
  matrix products  5.33 us (4%)
  local copies, waits for them, and re-layouts  5.09 us (4%)
  other arithmetic  1.74 us (1%)
    pallas_call x1, Pallas kernels, fused(): pl.pallas_call(functools.partial(fused_kernel, experts), out_shape=(jax.S...  126 us
    dot_general x2, matrix products, per_device(): picked = jnp.dot(picker, returned_rows, preferred_element_type=jnp.float32)  3.29 us

profile of v2, /device:TPU:0, one launch (start us, length us, event | category | flops | bytes accessed | tf_op | source)
XLA Modules:
  0.0 139.4 jit_solution(12677397436680483396)
XLA Ops:
  0.7 0.1 broadcast_multiply_fusion.1
  0.7 0.1 fusion.15
  0.9 1.1 copy.50
  2.0 0.1 bitcast_reduce_fusion
  2.1 0.7 mul.271
  2.8 0.1 multiply_multiply_fusion
  2.9 0.0 copy-start.3
  2.9 0.0 copy-start.8
  3.0 0.1 subtract_convert_fusion
  3.0 0.0 copy-start.4
  3.1 0.0 copy-start.6
  3.1 0.3 copy.53
  3.4 0.0 copy-start.1
  3.4 0.0 copy-start.5
  3.4 0.9 pad.4.clone
  4.4 0.0 copy-done.8
  4.4 0.1 fusion.10
  4.5 0.1 copy.49
  4.6 0.1 copy.48
  4.8 0.8 maximum_bitcast_fusion.kv
  5.5 0.1 copy.46
  5.7 0.1 eq.63
  5.8 0.2 fusion.2
  6.0 0.1 convert_element_type.76
  6.2 0.1 copy.47
  6.2 0.1 convert_reduce_fusion
  6.3 0.2 fusion.3
  6.5 1.8 %convolution_convert_fusion = bf16[384,2048]{1,0:T(8,128)(2,1)} fusion(bf16[128,2048]{1,0:T(8,128)(2,1)S(1)} %copy-done.1, f32[2048]{0:T(1024)S(1)} %copy-done.5, f32[128]{0:T(128)S(1)} %add_rsqrt_fusion.2, bf16[384,128]{1,0:T(8,128)(2,1)S(1)} %convert_reduce_fusion), kind=kOutput, calls=%fused_computation | convolution fusion | flops 203161600 | bytes 2204160 | tf_op jit(solution)/shard_map/dot_general | solution.py:371
  8.3 126.3 %fused.1 = (bf16[8,48,2048]{2,1,0:T(8,128)(2,1)}, bf16[128,2048]{1,0:T(8,128)(2,1)}) custom-call(bf16[8,48,2048]{2,1,0:T(8,128)(2,1)} %bitcast.37, bf16[2,256,128]{2,1,0:T(8,128)(2,1)} %maximum_bitcast_fusion.kv, bf16[2,1024,128]{2,1,0:T(8,128)(2,1)} %bitcast.39, bf16[256,2048]{1,0:T(8,128)(2,1)} %out_weight.1, bf16[2048,256]{1,0:T(8,128)(2,1)} %bitcast.40, ...), custom_call_target="tpu_custom_call" | custom-call | tf_op jit(solution)/shard_map/fused/pallas_call | solution.py:301
  134.7 2.0 %convolution_multiply_fusion.1 = f32[128,2048]{1,0:T(8,128)S(1)} fusion(bf16[384,2048]{1,0:T(8,128)(2,1)} %bitcast.35, f32[128]{0:T(128)S(1)} %get-tuple-element.15, s32[128]{0:T(128)S(1)} %get-tuple-element.13), kind=kOutput, calls=%fused_computation.3 | convolution fusion | flops 201637888 | bytes 2622464 | tf_op jit(solution)/shard_map/dot_general | solution.py:393
  136.7 1.3 fusion.1
  138.0 1.3 copy.55
  (24 shorter events, 0.2 us)
Async XLA Ops:
  2.9 1.4 copy-start.3
  2.9 1.4 %copy-start.8 = (f32[64]{0:T(128)S(1)}, f32[64]{0:T(128)}, u32[]{:S(2)}) copy-start(f32[64]{0:T(128)} %param.17) | copy-start | bytes 772
  3.0 1.6 %copy-start.4 = (bf16[256,2,64]{0,2,1:T(8,128)(2,1)S(1)}, bf16[256,2,64]{0,2,1:T(8,128)(2,1)}, u32[]{:S(2)}) copy-start(bf16[256,2,64]{0,2,1:T(8,128)(2,1)} %param.15) | copy-start | bytes 196612
  3.1 2.4 %copy-start.6 = (s32[128,2]{0,1:T(2,128)S(1)}, s32[128,2]{0,1:T(2,128)}, u32[]{:S(2)}) copy-start(s32[128,2]{0,1:T(2,128)} %param.21) | copy-start | bytes 3076
  3.4 2.9 %copy-start.1 = (bf16[128,2048]{1,0:T(8,128)(2,1)S(1)}, bf16[128,2048]{1,0:T(8,128)(2,1)}, u32[]{:S(2)}) copy-start(bf16[128,2048]{1,0:T(8,128)(2,1)} %param.19) | copy-start | bytes 1572868
  3.4 3.1 %copy-start.5 = (f32[2048]{0:T(1024)S(1)}, f32[2048]{0:T(1024)}, u32[]{:S(2)}) copy-start(f32[2048]{0:T(1024)} %param.20) | copy-start | bytes 24580
  8.3 126.4 %copy-start.7 = (f32[128,2]{0,1:T(2,128)S(1)}, f32[128,2]{0,1:T(2,128)}, u32[]{:S(2)}) copy-start(f32[128,2]{0,1:T(2,128)} %param.22) | copy-start | bytes 3076
  134.7 2.1 %copy-start = (bf16[8,48,2048]{2,1,0:T(8,128)(2,1)S(1)}, bf16[8,48,2048]{2,1,0:T(8,128)(2,1)}, u32[]{:S(2)}) copy-start(bf16[8,48,2048]{2,1,0:T(8,128)(2,1)} %get-tuple-element.5) | copy-start | bytes 4718596
  136.7 1.3 copy-start.2

commit v3 on v2

--- a/solution.py
+++ b/solution.py
@@ -145,8 +145,8 @@
     own_chunk.start()
     own_kv = pltpu.make_async_copy(kv, kv_all.at[e], own.at[1])
     own_kv.start()
+    lax.fori_loop(1, experts, lambda k, c: (chunk(k).start(), c)[1], 0)
     lax.fori_loop(1, half, lambda k, c: (kv_direct(k).start(), c)[1], 0)
-    lax.fori_loop(1, experts, lambda k, c: (chunk(k).start(), c)[1], 0)
     best[...] = jnp.full_like(best, -1e30)
     total[...] = jnp.zeros_like(total)
     accum[...] = jnp.zeros_like(accum)
@@ -164,31 +164,6 @@
             across(k).start()
             beside(k).start()
 
-        @pl.when((k >= 1) & (k < half))
-        def _():
-            kv_direct(k).wait_recv()
-            kv_side(k).start()
-
-        @pl.when((k >= half) & (k < experts))
-        def _():
-            kv_side(k - half).wait_recv()
-
-        @pl.when(k < experts)
-        def _():
-            direct = (e - 2 * k + 2 * experts) % experts
-            beyond = (side - 2 * (k - half) + 2 * experts) % experts
-            near = (experts + half - 1 - k) // experts
-            attend(near * direct + (1 - near) * beyond)
-
-        @pl.when(k == experts)
-        def _():
-            project()
-
-        @pl.when(k == experts + 1)
-        def _():
-            other(1).start()
-            other(0).start()
-
         @pl.when((k >= 2) & (k < experts + 2))
         def _():
             across(k - 2).wait_recv()
@@ -215,33 +190,59 @@
             pair_far(j).wait_recv()
             gone[j] = (part[high, j].astype(f32) + pair[1, j].astype(f32)).astype(bf16)
 
-        @pl.when(k == experts + 6)
+        @pl.when(k == experts + 7)
         def _():
             other(1).wait_recv()
             gone_att[...] = (prod[high].astype(f32) + pair_att[1].astype(f32)).astype(bf16)
 
-        @pl.when(k == experts + 7)
+        @pl.when(k == experts + 9)
         def _():
             other(2).start()
 
-        @pl.when(k == 9)
+        @pl.when(k == 10)
         def _():
             pltpu.make_async_copy(done.at[0], ret.at[e], own.at[0]).start()
 
-        @pl.when((k >= 10) & (k < experts + 9))
-        def _():
-            back(k - 9).start()
-
-        @pl.when((k >= 8) & (k < experts + 8))
-        def _():
-            j = k - 8
+        @pl.when((k >= 11) & (k < experts + 10))
+        def _():
+            back(k - 10).start()
+
+        @pl.when((k >= 9) & (k < experts + 9))
+        def _():
+            j = k - 9
             pair_near(j).wait_recv()
             over(j).wait_recv()
             done[j] = (part[t, j].astype(f32) + pair[0, j].astype(f32) + seen[j].astype(f32)).astype(bf16)
 
+        @pl.when((k >= 6) & (k < half + 5))
+        def _():
+            kv_direct(k - 5).wait_recv()
+            kv_side(k - 5).start()
+
+        @pl.when((k >= half + 5) & (k < experts + 5))
+        def _():
+            kv_side(k - 5 - half).wait_recv()
+
+        @pl.when((k >= 5) & (k < experts + 5))
+        def _():
+            i = k - 5
+            direct = (e - 2 * i + 2 * experts) % experts
+            beyond = (side - 2 * (i - half) + 2 * experts) % experts
+            near = (experts + half - 1 - i) // experts
+            attend(near * direct + (1 - near) * beyond)
+
+        @pl.when(k == experts + 5)
+        def _():
+            project()
+
+        @pl.when(k == experts + 6)
+        def _():
+            other(1).start()
+            other(0).start()
+
         return carry
 
-    lax.fori_loop(0, experts + 9, step, 0)
+    lax.fori_loop(0, experts + 10, step, 0)
     other(0).wait_recv()
     other(2).wait_recv()
     att[...] = (prod[t].astype(f32) + pair_att[0].astype(f32) + seen_att[...].astype(f32)).astype(bf16)

time: 140 us -> 128 us (0.914)
  Pallas kernels: 126 us -> 115 us
    pallas_call x1, Pallas kernels: 126 us -> 115 us  [fused(): pl.pallas_call(functools.partial(fused_kernel, experts), out_shape=(jax.S...]
where the time goes in v3:
time: 128 us
  Pallas kernels  115 us (90%)
  matrix products  5.33 us (4%)
  local copies, waits for them, and re-layouts  5.09 us (4%)
  other arithmetic  1.74 us (1%)
    pallas_call x1, Pallas kernels, fused(): pl.pallas_call(functools.partial(fused_kernel, experts), out_shape=(jax.S...  115 us
    dot_general x2, matrix products, per_device(): picked = jnp.dot(picker, returned_rows, preferred_element_type=jnp.float32)  3.3 us

profile of v3, /device:TPU:0, one launch (start us, length us, event | category | flops | bytes accessed | tf_op | source)
XLA Modules:
  0.0 127.9 jit_solution(1512589419353581769)
XLA Ops:
  0.7 0.1 broadcast_multiply_fusion.1
  0.7 0.1 fusion.15
  0.9 1.1 copy.50
  2.0 0.1 bitcast_reduce_fusion
  2.1 0.7 mul.271
  2.8 0.1 multiply_multiply_fusion
  2.9 0.0 copy-start.3
  2.9 0.0 copy-start.8
  3.0 0.1 subtract_convert_fusion
  3.0 0.0 copy-start.4
  3.1 0.0 copy-start.6
  3.1 0.3 copy.53
  3.4 0.0 copy-start.1
  3.4 0.0 copy-start.5
  3.4 0.9 pad.4.clone
  4.3 0.0 copy-done.3
  4.4 0.1 fusion.10
  4.5 0.1 copy.49
  4.6 0.1 copy.48
  4.8 0.8 maximum_bitcast_fusion.kv
  5.5 0.1 copy.46
  5.7 0.1 eq.63
  5.8 0.2 fusion.2
  6.0 0.1 convert_element_type.76
  6.2 0.1 copy.47
  6.2 0.1 convert_reduce_fusion
  6.3 0.2 fusion.3
  6.5 1.8 %convolution_convert_fusion = bf16[384,2048]{1,0:T(8,128)(2,1)} fusion(bf16[128,2048]{1,0:T(8,128)(2,1)S(1)} %copy-done.1, f32[2048]{0:T(1024)S(1)} %copy-done.5, f32[128]{0:T(128)S(1)} %add_rsqrt_fusion.2, bf16[384,128]{1,0:T(8,128)(2,1)S(1)} %convert_reduce_fusion), kind=kOutput, calls=%fused_computation | convolution fusion | flops 203161600 | bytes 2204160 | tf_op jit(solution)/shard_map/dot_general | solution.py:372
  8.3 114.8 %fused.1 = (bf16[8,48,2048]{2,1,0:T(8,128)(2,1)}, bf16[128,2048]{1,0:T(8,128)(2,1)}) custom-call(bf16[8,48,2048]{2,1,0:T(8,128)(2,1)} %bitcast.37, bf16[2,256,128]{2,1,0:T(8,128)(2,1)} %maximum_bitcast_fusion.kv, bf16[2,1024,128]{2,1,0:T(8,128)(2,1)} %bitcast.39, bf16[256,2048]{1,0:T(8,128)(2,1)} %out_weight.1, bf16[2048,256]{1,0:T(8,128)(2,1)} %bitcast.40, ...), custom_call_target="tpu_custom_call" | custom-call | tf_op jit(solution)/shard_map/fused/pallas_call | solution.py:302
  123.2 2.0 %convolution_multiply_fusion.1 = f32[128,2048]{1,0:T(8,128)S(1)} fusion(bf16[384,2048]{1,0:T(8,128)(2,1)} %bitcast.35, f32[128]{0:T(128)S(1)} %get-tuple-element.15, s32[128]{0:T(128)S(1)} %get-tuple-element.13), kind=kOutput, calls=%fused_computation.3 | convolution fusion | flops 201637888 | bytes 2622464 | tf_op jit(solution)/shard_map/dot_general | solution.py:394
  125.2 1.3 %fusion.1 = bf16[128,2048]{1,0:T(8,128)(2,1)} fusion(f32[128,2048]{1,0:T(8,128)S(1)} %convolution_multiply_fusion.1, bf16[384,2048]{1,0:T(8,128)(2,1)S(1)} %bitcast.36, f32[128]{0:T(128)S(1)} %get-tuple-element.14, s32[128]{0:T(128)S(1)} %get-tuple-element.12), kind=kOutput, calls=%fused_computation.4 | convolution fusion | flops 202162176 | bytes 3146752 | tf_op jit(solution)/shard_map/dot_general | solution.py:394
  126.5 1.3 %copy.55 = bf16[2,64,2048]{2,0,1:T(2,128)(2,1)} copy(bf16[2,64,2048]{2,1,0:T(8,128)(2,1)S(1)} %bitcast.45) | data formatting | bytes 1048576 | tf_op jit(solution)/shard_map/reshape | solution.py:390
  (24 shorter events, 0.2 us)
Async XLA Ops:
  2.9 1.4 %copy-start.3 = (bf16[256,2,64]{0,2,1:T(8,128)(2,1)S(1)}, bf16[256,2,64]{0,2,1:T(8,128)(2,1)}, u32[]{:S(2)}) copy-start(bf16[256,2,64]{0,2,1:T(8,128)(2,1)} %param.14) | copy-start | bytes 196612
  2.9 1.4 %copy-start.8 = (f32[64]{0:T(128)S(1)}, f32[64]{0:T(128)}, u32[]{:S(2)}) copy-start(f32[64]{0:T(128)} %param.17) | copy-start | bytes 772
  3.0 1.6 %copy-start.4 = (bf16[256,2,64]{0,2,1:T(8,128)(2,1)S(1)}, bf16[256,2,64]{0,2,1:T(8,128)(2,1)}, u32[]{:S(2)}) copy-start(bf16[256,2,64]{0,2,1:T(8,128)(2,1)} %param.15) | copy-start | bytes 196612
  3.1 2.4 %copy-start.6 = (s32[128,2]{0,1:T(2,128)S(1)}, s32[128,2]{0,1:T(2,128)}, u32[]{:S(2)}) copy-start(s32[128,2]{0,1:T(2,128)} %param.21) | copy-start | bytes 3076
  3.4 2.9 %copy-start.1 = (bf16[128,2048]{1,0:T(8,128)(2,1)S(1)}, bf16[128,2048]{1,0:T(8,128)(2,1)}, u32[]{:S(2)}) copy-start(bf16[128,2048]{1,0:T(8,128)(2,1)} %param.19) | copy-start | bytes 1572868
  3.4 3.1 %copy-start.5 = (f32[2048]{0:T(1024)S(1)}, f32[2048]{0:T(1024)}, u32[]{:S(2)}) copy-start(f32[2048]{0:T(1024)} %param.20) | copy-start | bytes 24580
  8.3 114.8 %copy-start.7 = (f32[128,2]{0,1:T(2,128)S(1)}, f32[128,2]{0,1:T(2,128)}, u32[]{:S(2)}) copy-start(f32[128,2]{0,1:T(2,128)} %param.22) | copy-start | bytes 3076
  123.2 2.1 %copy-start = (bf16[8,48,2048]{2,1,0:T(8,128)(2,1)S(1)}, bf16[8,48,2048]{2,1,0:T(8,128)(2,1)}, u32[]{:S(2)}) copy-start(bf16[8,48,2048]{2,1,0:T(8,128)(2,1)} %get-tuple-element.5) | copy-start | bytes 4718596
  125.2 1.3 %copy-start.2 = (bf16[128,2048]{1,0:T(8,128)(2,1)S(1)}, bf16[128,2048]{1,0:T(8,128)(2,1)}, u32[]{:S(2)}) copy-start(bf16[128,2048]{1,0:T(8,128)(2,1)} %get-tuple-element.4) | copy-start | bytes 1572868
